TPU v7x, 256 devices: a whole 4x4x8 slice. The times are simulated.
256 devices in a mesh: ep: 64 (over z, x, core), tp: 4 (over y).
Axes of the slice: x: 4, y: 4, z: 8, core: 2. Of those that a mesh axis runs over, the one named last changes fastest.
Arguments:
- queries: bfloat16 [16384, 8, 128], P('ep', 'tp'), may hold values from -256 to 256
- keys: bfloat16 [16384, 4, 128], P('ep', 'tp'), may hold values from -8 to 8
- values: bfloat16 [16384, 4, 128], P('ep', 'tp'), may hold values from -6 to 6
- attn_lambda: float32 [8], P('tp'), may hold values from 0.3 to 0.8
- head_gain: float32 [128], replicated, may hold values from 0.1 to 1.9
- w_out: bfloat16 [1024, 2048], replicated, may hold values from -0.1875 to 0.1875
- moe_rows: bfloat16 [32768, 2048], P('ep'), may hold values from -6 to 6
- moe_gain: float32 [2048], replicated, may hold values from 0.1 to 1.9
- routes: int32 [32768, 2], P('ep'), may hold values from 0 to 63, all different within a row; in each aligned block of 128 rows (0 to 127, 128 to 255, ...) at most 8 rows name the same one
- route_weights: float32 [32768, 2], P('ep'), may hold values from 0.1 to 1
- w_gate: bfloat16 [64, 2048, 1024], P('ep', None, 'tp'), may hold values from -0.125 to 0.125
- w_up: bfloat16 [64, 2048, 1024], P('ep', None, 'tp'), may hold values from -0.125 to 0.125
- w_down: bfloat16 [64, 1024, 2048], P('ep', 'tp'), may hold values from -0.1875 to 0.1875
Outputs:
- mixer_out: bfloat16 [16384, 2048], P(('ep', 'tp'))
- moe_out: bfloat16 [32768, 2048], P(('ep', 'tp'))
Inputs may be any that keep to these rules, and one draw needn't show every extreme that they name: `routes`: each row names 2 different experts. In each aligned block of 128 rows (the rows of moe_out that one device holds) no expert is named by more than 8 rows, a bound that some block reaches.
All inputs are finite; a program needn't handle non-finite values.
Results may differ from a plain program's by a relative error of at most 0.011.
Values may be sent and summed in bfloat16 or wider, within the bound.
No kernel may reach another device: no remote copies, remote signals or barrier semaphores. Data moves between devices by JAX's collectives and lax.ppermute only.
A program may use at most 128 MiB of HBM per device.

v0:
```python
import jax
import jax.numpy as jnp
from jax import lax
from jax.sharding import PartitionSpec as P

EPSILON = 1e-06
MASKED = -1e30


def split_up(x, dim, size):
    before, after = (x.shape[:dim], x.shape[dim + 1 :])
    return jnp.moveaxis(x.reshape(*before, size, -1, *after), dim, 0)


def sum_at_owner(x, axis, dim):
    size = lax.axis_size(axis)
    tiles = lax.all_to_all(split_up(x, dim, size), axis, 0, 0, tiled=True)
    return jnp.sum(tiles.astype(jnp.float32), axis=0)


def joined_along(tiles, dim):
    tiles = jnp.moveaxis(tiles, 0, dim)
    lengths = tiles.shape
    return tiles.reshape(*lengths[:dim], lengths[dim] * lengths[dim + 1], *lengths[dim + 2 :])


def piecewise(x, axis, dim, work, out_dim):
    span = x.shape[dim]
    pieces = jnp.split(x, 2, axis=dim) if span % 2 == 0 else [x]
    first = jnp.arange(lax.axis_size(axis)) * span
    tiles = [lax.all_gather(section, axis) for section in pieces]
    made = [jax.vmap(work)(b, first + k * (span // len(pieces))) for k, b in enumerate(tiles)]
    return joined_along(jnp.concatenate(made, axis=out_dim + 1), out_dim)


def rms_scaled(values_f, gain):
    mean_sq = jnp.mean(values_f * values_f, axis=-1, keepdims=True)
    return values_f * lax.rsqrt(mean_sq + EPSILON) * gain


def slot_numbers(block_routes, experts):
    flat_ids = block_routes.reshape(-1)
    matches = (flat_ids[:, None] == lax.iota(jnp.int32, experts)[None, :]).astype(jnp.int32)
    earlier = jnp.cumsum(matches, axis=0) - matches
    return jnp.sum(earlier * matches, axis=1).reshape(block_routes.shape)


def fill_slots(block_rows, block_routes, experts, capacity):
    slot_ids = slot_numbers(block_routes, experts)
    model_width = block_rows.shape[1]
    copies = jnp.broadcast_to(block_rows[:, None, :], block_routes.shape + (model_width,))
    blank_slots = jnp.zeros((experts, capacity, model_width), block_rows.dtype)
    return (blank_slots.at[block_routes, slot_ids].set(copies), slot_ids)


def local(
    queries,
    keys,
    values,
    attn_lambda,
    head_gain,
    w_out,
    moe_rows,
    moe_gain,
    routes,
    route_weights,
    w_gate,
    w_up,
    w_down,
):
    positions = queries.shape[0]
    q_heads = queries.shape[1]
    kv_heads = keys.shape[1]
    head_dim = queries.shape[2] // 2
    value_dim = values.shape[2]
    per_key = q_heads // kv_heads
    first_pos = lax.axis_index("ep") * positions
    query_pos = first_pos + lax.iota(jnp.int32, positions)
    last_pos = first_pos + positions - 1
    query_view = queries.reshape(positions, kv_heads, per_key, 2, head_dim)
    inv_scale = head_dim ** (-0.5)
    start_max = jnp.full((positions, kv_heads, per_key, 2), MASKED, jnp.float32)
    start_total = jnp.zeros((positions, kv_heads, per_key, 2), jnp.float32)
    start_acc = jnp.zeros((positions, kv_heads, per_key, 2, value_dim), jnp.float32)
    carry = (start_max, start_total, start_acc)
    key_piece = lax.all_gather(keys, "ep", axis=0, tiled=True)
    value_piece = lax.all_gather(values, "ep", axis=0, tiled=True)
    shard_count = key_piece.shape[0] // positions
    together = 1
    for candidate in (2, 3, 4):
        if shard_count % candidate == 0:
            together = candidate
    block_len = together * positions
    blocks = shard_count // together
    key_blocks = key_piece.reshape(blocks, block_len, kv_heads, 2, head_dim)
    value_blocks = value_piece.reshape(blocks, block_len, kv_heads, value_dim)
    block_starts = block_len * lax.iota(jnp.int32, blocks)

    def visit(running, inputs):
        key_blk, value_blk, block_start = inputs

        def update(current):
            run_max, run_total, run_acc = current
            key_pos = block_start + lax.iota(jnp.int32, block_len)
            scores = (
                jnp.einsum(
                    "qkgmd,pkmd->qkgmp", query_view, key_blk, preferred_element_type=jnp.float32
                )
                * inv_scale
            )
            allowed = key_pos[None, :] <= query_pos[:, None]
            scores = jnp.where(allowed[:, None, None, None, :], scores, MASKED)
            new_max = jnp.maximum(run_max, jnp.max(scores, axis=-1))
            shrink = jnp.exp(run_max - new_max)
            weights = jnp.exp(scores - new_max[..., None])
            run_total = run_total * shrink + jnp.sum(weights, axis=-1)
            run_acc = run_acc * shrink[..., None] + jnp.einsum(
                "qkgmp,pkv->qkgmv",
                weights.astype(jnp.bfloat16),
                value_blk,
                preferred_element_type=jnp.float32,
            )
            return (new_max, run_total, run_acc)

        def keep(current):
            return current

        return (lax.cond(block_start <= last_pos, update, keep, running), None)

    carry, unused = lax.scan(visit, carry, (key_blocks, value_blocks, block_starts))
    run_max, run_total, run_acc = carry
    ratios = run_acc / run_total[..., None]
    lambda_view = attn_lambda.reshape(1, kv_heads, per_key, 1)
    head_out = ratios[:, :, :, 0] - lambda_view * ratios[:, :, :, 1]
    attn_rows = (
        rms_scaled(head_out, head_gain).astype(jnp.bfloat16).reshape(positions, q_heads * value_dim)
    )
    tp_count = lax.axis_size("tp")
    tp_id = lax.axis_index("tp")
    head_width = q_heads * value_dim
    w_local = lax.dynamic_slice_in_dim(w_out, tp_id * head_width, head_width, 0)
    mixer_out = sum_at_owner(
        jnp.dot(attn_rows, w_local, preferred_element_type=jnp.float32).astype(jnp.bfloat16),
        "tp",
        0,
    ).astype(jnp.bfloat16)
    experts = lax.axis_size("ep")
    dev_rows = moe_rows.shape[0] // tp_count
    top_count = routes.shape[1]
    capacity = max(2, 2 * dev_rows * top_count // experts)
    model_width = moe_rows.shape[1]
    hidden_units = w_gate.shape[2]
    own_routes = lax.dynamic_slice_in_dim(routes, tp_id * dev_rows, dev_rows, 0)
    own_weights = lax.dynamic_slice_in_dim(route_weights, tp_id * dev_rows, dev_rows, 0)

    def expert_hidden(slot_rows):
        flat_rows = slot_rows.reshape(-1, model_width)
        gate_out = jnp.dot(flat_rows, w_gate[0], preferred_element_type=jnp.float32)
        up_out = jnp.dot(flat_rows, w_up[0], preferred_element_type=jnp.float32)
        return (
            (jax.nn.silu(gate_out) * up_out)
            .astype(jnp.bfloat16)
            .reshape(slot_rows.shape[:-1] + (hidden_units,))
        )

    own_rows = rms_scaled(
        lax.dynamic_slice_in_dim(moe_rows, tp_id * dev_rows, dev_rows, 0).astype(jnp.float32),
        moe_gain,
    ).astype(jnp.bfloat16)
    outgoing, own_slots = fill_slots(own_rows, own_routes, experts, capacity)
    arrived = lax.all_to_all(outgoing, "ep", split_axis=0, concat_axis=0, tiled=True)

    def hidden_piece(slot_rows, begin_row):
        return expert_hidden(slot_rows)

    hidden = piecewise(arrived[None], "tp", 0, hidden_piece, 0)
    all_units = lax.all_to_all(hidden, "tp", split_axis=0, concat_axis=3, tiled=True)
    down_whole = lax.all_gather(w_down[0], "tp", axis=0, tiled=True)
    flat_units = all_units.reshape(-1, tp_count * hidden_units)
    summed_f = jnp.zeros((flat_units.shape[0], model_width), jnp.float32)
    for group in range(tp_count):
        unit_block = flat_units[:, group * hidden_units : (group + 1) * hidden_units]
        weight_block = down_whole[group * hidden_units : (group + 1) * hidden_units]
        group_part = jnp.dot(unit_block, weight_block, preferred_element_type=jnp.float32).astype(
            jnp.bfloat16
        )
        summed_f = summed_f + group_part.astype(jnp.float32)
    summed = summed_f.astype(jnp.bfloat16).reshape(all_units.shape[:-1] + (model_width,))
    returned = lax.all_to_all(summed, "ep", split_axis=1, concat_axis=1, tiled=True)[0]
    picked = returned[own_routes, own_slots]
    moe_out = jnp.sum(own_weights[..., None] * picked.astype(jnp.float32), axis=1).astype(
        jnp.bfloat16
    )
    return (mixer_out, moe_out)


def solution(mesh):
    return jax.shard_map(
        local,
        mesh=mesh,
        in_specs=(
            P("ep", "tp", None),
            P("ep", "tp", None),
            P("ep", "tp", None),
            P("tp"),
            P(),
            P(),
            P("ep", None),
            P(),
            P("ep", None),
            P("ep", None),
            P("ep", None, "tp"),
            P("ep", None, "tp"),
            P("ep", "tp", None),
        ),
        out_specs=(P(("ep", "tp"), None), P(("ep", "tp"), None)),
        check_vma=False,
    )
```

profile of v0, /device:TPU:2, one launch (start us, length us, event | category | flops | bytes accessed | tf_op | source)
XLA Modules:
  0.0 434.8 jit_solution(10305571413842020620)
XLA Ops:
  7.2 0.7 all-gather.7.cloned.1.call-update
  8.0 0.7 all-gather.9.cloned.1.call-update
  8.7 0.7 constant_dynamic-slice_fusion
  9.8 0.6 reduce-window.6
  11.1 1.2 fusion.25
  12.3 1.3 fusion.27
  13.6 0.6 broadcast_in_dim.57
  14.2 1.2 reshape.247
  15.7 33.0 %scatter_fusion = bf16[64,8,2048]{2,1,0:T(8,128)(2,1)S(1)} fusion(bf16[64,8,2048]{2,1,0:T(8,128)(2,1)S(1)} %broadcast_in_dim.36, s32[256]{0:T(256)S(1)} %reshape.245, bf16[256,2048]{1,0:T(8,128)(2,1)} %reshape.247), kind=kCustom, calls=%fused_computation.1 | custom fusion | bytes 3147776 | tf_op jit(solution)/shard_map/scatter | solution.py:53
  48.8 73.1 %all_to_all.30 = bf16[64,8,2048]{2,1,0:T(8,128)(2,1)} all-to-all(bf16[64,8,2048]{2,1,0:T(8,128)(2,1)S(1)} %scatter_fusion), channel_id=1, replica_groups=mesh['ep'=64,'tp'=4] {'ep'}, dimensions={0} | all-to-all | bytes 4194304 | tf_op jit(solution)/shard_map/all_to_all | solution.py:171
  122.7 14.7 %reshape.263 = bf16[16,1024,1,2,64]{4,3,1,0,2:T(2,128)(2,1)} reshape(bf16[16384,1,128]{2,0,1:T(8,128)(2,1)} %all-gather.7.cloned.1.call-done) | data formatting | bytes 8388608 | tf_op jit(solution)/shard_map/reshape | solution.py:95
  137.4 20.2 %copy.37 = bf16[16,1024,1,2,64]{1,4,3,2,0:T(8,128)(2,1)} copy(bf16[16,1024,1,2,64]{4,3,1,0,2:T(2,128)(2,1)} %reshape.263) | data formatting | bytes 8388608
  157.6 29.6 %all-gather.9.cloned.1.call-done = bf16[16384,1,128]{2,0,1:T(8,128)(2,1)} async-done(((bf16[256,1,128]{2,0,1:T(8,128)(2,1)}), bf16[16384,1,128]{2,0,1:T(8,128)(2,1)}) %all-gather.9.cloned.1.call-update) | async-done | bytes 4194320 | tf_op jit(solution)/shard_map/all_gather | solution.py:87
  187.2 6.4 %copy.39 = bf16[16,1024,1,128]{1,3,2,0:T(8,128)(2,1)} copy(bf16[16,1024,1,128]{3,1,0,2:T(8,128)(2,1)} %bitcast.160) | data formatting | bytes 8388608
  193.6 23.8 %while.15 = (s32[]{:T(128)}, f32[256,1,2,2]{0,2,3,1:T(2,128)S(1)}, f32[256,1,2,2]{0,2,3,1:T(2,128)S(1)}, f32[256,1,2,2,128]{0,4,3,2,1:T(8,128)S(1)}, s32[16]{0:T...) while((s32[]{:T(128)}, f32[256,1,2,2]{0,2,3,1:T(2,128)S(1)}, ...), condition=%wide.region_5.6_spmd.clone, body=%wide.region_0.5_spmd.clone.sunk | while | flops 411570432 | bytes 15156511 | solution.py:130
  193.7 0.6 dynamic_slice.56
  194.8 5.2 %conditional.3 = ((f32[256,1,2,2]{0,2,3,1:T(2,128)S(1)}, f32[256,1,2,2]{0,2,3,1:T(2,128)S(1)}, f32[256,1,2,2,128]{0,4,3,2,1:T(8,128)S(1)})) conditional(s32[]{:T(128)} %convert_element_type.131, (f32[256,1,2,2]{0,2,3,1:T(2,128)S(1)}, f32[256,1,2,2]{0,2,3,1:T(2,128)S(1)}, f32[256,1,2,2,128]{0,4,3,2,1:T(8,128)S(1)}) %tuple.48, (s32[]{:T(128)}, ...), branch_computations={%region_1.1_spmd, %region_2.4_spmd} | conditional | flops 411570432 | bytes 15155240 | solution.py:128
  195.6 1.8 fusion.4
  197.4 1.0 fusion.5
  198.5 1.5 fusion.11
  200.0 0.6 dynamic_slice.56
  201.2 0.6 dynamic_slice.56
  202.3 0.6 dynamic_slice.56
  203.5 0.6 dynamic_slice.56
  204.7 0.6 dynamic_slice.56
  207.0 0.6 dynamic_slice.56
  208.2 0.6 dynamic_slice.56
  217.5 55.6 %all-gather.11.cloned.1.call-done = bf16[256,8,2048]{2,1,0:T(8,128)(2,1)} async-done(((bf16[64,8,2048]{2,1,0:T(8,128)(2,1)}), bf16[256,8,2048]{2,1,0:T(8,128)(2,1)}) %all-gather.11.cloned.1.call-update) | async-done | bytes 8388624 | tf_op jit(solution)/shard_map/all_gather | solution.py:31
  273.1 5.9 %fusion.28 = f32[4,512,256]{2,1,0:T(8,128)S(1)} fusion(bf16[4,512,2048]{2,1,0:T(8,128)(2,1)} %bitcast.170, bf16[1,2048,256]{2,1,0:T(8,128)(2,1)S(1)} %copy-done), kind=kOutput, calls=%fused_computation.47 | convolution fusion | flops 2147483648 | bytes 11534336 | tf_op jit(solution)/shard_map/vmap()/dot_general | solution.py:159
  279.1 3.6 fusion.24
  282.7 4.0 all-to-all-start.2
  287.0 2.8 convolution_convert_fusion.4
  289.8 22.2 %all-to-all-done.2 = bf16[4,64,8,256]{3,2,1,0:T(8,128)(2,1)S(1)} async-done(((bf16[4,64,8,256]{3,2,1,0:T(8,128)(2,1)}), bf16[4,64,8,256]{3,2,1,0:T(8,128)(2,1)S(1)}, u32[]{:S(2)}, u32[]{:S(2)}) %all-to-all-start.2) | async-done | bytes 1048608 | tf_op jit(solution)/shard_map/all_to_all | solution.py:177
  312.0 3.7 all-to-all-start
  315.7 1.4 copy.65
  317.3 29.3 %all-gather.13.cloned.1.call-done = bf16[1,1024,2048]{2,1,0:T(8,128)(2,1)} async-done(((bf16[1,256,2048]{2,1,0:T(8,128)(2,1)}), bf16[1,1024,2048]{2,1,0:T(8,128)(2,1)}) %all-gather.13.cloned.1.call-update) | async-done | bytes 4194320 | tf_op jit(solution)/shard_map/all_gather | solution.py:178
  346.6 2.1 convolution_convert_fusion
  348.7 1.9 convolution_convert_fusion.1
  350.7 0.7 convolution_convert_fusion.2
  351.4 2.6 fusion.23
  354.0 1.0 copy-done.2
  355.0 10.6 %all-to-all-start.3 = ((bf16[1,64,8,2048]{3,2,0,1:T(8,128)(2,1)}), bf16[1,64,8,2048]{3,2,0,1:T(8,128)(2,1)S(1)}, u32[]{:S(2)}, u32[]{:S(2)}) async-start(bf16[1,64,8,2048]{3,2,0,1:T(8,128)(2,1)} %fusion.23), calls=%async_computation.3 | async-start | bytes 4194304 | tf_op jit(solution)/shard_map/all_to_all | solution.py:189
  365.7 0.7 constant_dynamic-slice_fusion.1
  366.5 2.2 reduce_sum.60
  368.7 48.1 %all-to-all-done.3 = bf16[1,64,8,2048]{3,2,0,1:T(8,128)(2,1)S(1)} async-done(((bf16[1,64,8,2048]{3,2,0,1:T(8,128)(2,1)}), bf16[1,64,8,2048]{3,2,0,1:T(8,128)(2,1)S(1)}, u32[]{:S(2)}, u32[]{:S(2)}) %all-to-all-start.3) | async-done | bytes 2097184 | tf_op jit(solution)/shard_map/all_to_all | solution.py:189
  416.8 5.2 %gather_fusion = bf16[256,2048]{1,0:T(8,128)(2,1)} fusion(bf16[64,8,2048]{2,1,0:T(8,128)(2,1)S(1)} %bitcast.159, s32[256]{0:T(256)S(1)} %reshape.239), kind=kCustom, calls=%fused_computation | custom fusion | bytes 2099200 | tf_op jit(solution)/shard_map/gather | solution.py:190
  422.0 2.4 reshape.258
  424.4 3.9 multiply_reduce_fusion
  (98 shorter events, 8.7 us)
Async XLA Ops:
  7.2 266.0 %copy-start = (bf16[1,2048,256]{2,1,0:T(8,128)(2,1)S(1)}, bf16[1,2048,256]{2,1,0:T(8,128)(2,1)}, u32[]{:S(2)}) copy-start(bf16[1,2048,256]{2,1,0:T(8,128)(2,1)} %param.28) | copy-start | bytes 3145732
  7.2 115.6 %all-gather.7.cloned.1.call-start = ((), (), s32[]{:S(2)}) async-start(), calls=%async_computation.4 | async-start | bytes 4259840 | tf_op jit(solution)/shard_map/all_gather | solution.py:86
  7.9 179.3 %all-gather.9.cloned.1.call-start = ((), (), s32[]{:S(2)}) async-start(), calls=%async_computation.5 | async-start | bytes 4259840 | tf_op jit(solution)/shard_map/all_gather | solution.py:87
  8.7 264.5 %all-gather.11.cloned.1.call-start = ((), (), s32[]{:S(2)}) async-start(), calls=%async_computation.6 | async-start | bytes 10485760 | tf_op jit(solution)/shard_map/all_gather | solution.py:31
  48.7 73.8 %copy-start.3 = (bf16[256,2,128]{2,1,0:T(2,128)(2,1)S(1)}, bf16[256,2,128]{2,1,0:T(2,128)(2,1)}, u32[]{:S(2)}) copy-start(bf16[256,2,128]{2,1,0:T(2,128)(2,1)} %param.17) | copy-start | bytes 393220
  48.7 73.9 %copy-start.4 = (f32[2]{0:T(128)S(1)}, f32[2]{0:T(128)}, u32[]{:S(2)}) copy-start(f32[2]{0:T(128)} %param.20) | copy-start | bytes 28
  48.8 73.9 %copy-start.5 = (f32[128]{0:T(128)S(1)}, f32[128]{0:T(128)}, u32[]{:S(2)}) copy-start(f32[128]{0:T(128)} %param.21) | copy-start | bytes 1540
  121.9 224.7 %all-gather.13.cloned.1.call-start = ((), (), s32[]{:S(2)}) async-start(), calls=%async_computation.7 | async-start | bytes 5242880 | tf_op jit(solution)/shard_map/all_gather | solution.py:178
  273.1 5.9 %copy-start.6 = (bf16[256,8,2048]{2,1,0:T(8,128)(2,1)S(1)}, bf16[256,8,2048]{2,1,0:T(8,128)(2,1)}, u32[]{:S(2)}) copy-start(bf16[256,8,2048]{2,1,0:T(8,128)(2,1)} %all-gather.11.cloned.1.call-done) | copy-start | bytes 25165828
  273.1 6.0 %copy-start.7 = (bf16[1,2048,256]{2,1,0:T(8,128)(2,1)S(1)}, bf16[1,2048,256]{2,1,0:T(8,128)(2,1)}, u32[]{:S(2)}) copy-start(bf16[1,2048,256]{2,1,0:T(8,128)(2,1)} %param.27) | copy-start | bytes 3145732
  282.7 29.3 %all-to-all-start.2 = ((bf16[4,64,8,256]{3,2,1,0:T(8,128)(2,1)}), bf16[4,64,8,256]{3,2,1,0:T(8,128)(2,1)S(1)}, u32[]{:S(2)}, u32[]{:S(2)}) async-start(bf16[4,64,8,256]{3,2,1,0:T(8,128)(2,1)} %fusion.24), calls=%async_computation.2 | async-start | bytes 2097152 | tf_op jit(solution)/shard_map/all_to_all | solution.py:177
  312.0 42.0 %all-to-all-start = ((bf16[4,64,2048]{2,1,0:T(8,128)(2,1)}), bf16[4,64,2048]{2,1,0:T(8,128)(2,1)S(1)}, u32[]{:S(2)}, u32[]{:S(2)}) async-start(bf16[4,64,2048]{2,1,0:T(8,128)(2,1)} %bitcast.26), calls=%async_computation | async-start | bytes 2097152 | tf_op jit(solution)/shard_map/all_to_all | solution.py:17
  346.6 4.0 copy-start.1
  354.0 1.0 copy-start.2
  355.0 61.8 %all-to-all-start.3 = ((bf16[1,64,8,2048]{3,2,0,1:T(8,128)(2,1)}), bf16[1,64,8,2048]{3,2,0,1:T(8,128)(2,1)S(1)}, u32[]{:S(2)}, u32[]{:S(2)}) async-start(bf16[1,64,8,2048]{3,2,0,1:T(8,128)(2,1)} %fusion.23), calls=%async_computation.3 | async-start | bytes 4194304 | tf_op jit(solution)/shard_map/all_to_all | solution.py:189
Sparse Core Ops, SparseCore 0:
  10.8 94.4 all-gather.6
  108.0 79.1 all-gather.8
  189.0 84.0 all-gather.10
  274.8 71.7 all-gather.12
where the time goes:
time: 438 us; the launch traced here: 435 us
  waiting for transfers between devices  187 us (43%)
  local copies, waits for them, and re-layouts  98.3 us (22%)
  blocking collectives  73.1 us (17%)
  matrix products  23 us (5%)
  starting transfers between devices  18.6 us (4%)
  between operations  14.1 us (3%)
  other arithmetic  11.5 us (3%)
  loops' own time  9.72 us (2%)
    all_to_all x1, blocking collectives, local(): lax.all_to_all(outgoing, 'ep', split_axis=0, concat_axis=0, tiled=True)  73.1 us
    all_gather x1, waiting for transfers between devices, piecewise(): tiles = [lax.all_gather(section, axis) for section in pieces]  55.6 us
    all_to_all x1, waiting for transfers between devices, local(): lax.all_to_all(summed, 'ep', split_axis=1, concat_axis=1, tiled=True)[0]  48.1 us
    scatter x1, local copies, waits for them, and re-layouts, fill_slots(): return (blank_slots.at[block_routes, slot_ids].set(copies), slot_ids)  33 us
    all_gather x1, waiting for transfers between devices, local(): value_piece = lax.all_gather(values, 'ep', axis=0, tiled=True)  29.6 us
    all_gather x1, waiting for transfers between devices, local(): down_whole = lax.all_gather(w_down[0], 'tp', axis=0, tiled=True)  29.3 us
    unnamed x22, local copies, waits for them, and re-layouts  28.1 us
    all_to_all x1, waiting for transfers between devices, local(): lax.all_to_all(hidden, 'tp', split_axis=0, concat_axis=3, tiled=True)  22.2 us
  transfers between devices with their start and end apart: 7, of which 5 were waited for; matrix products, arithmetic and copies ran while one was open for 28% of the time, Pallas kernels for 0%

commit v1 on v0

--- a/solution.py
+++ b/solution.py
@@ -84,7 +84,10 @@
     start_acc = jnp.zeros((positions, kv_heads, per_key, 2, value_dim), jnp.float32)
     carry = (start_max, start_total, start_acc)
     key_piece = lax.all_gather(keys, "ep", axis=0, tiled=True)
-    value_piece = lax.all_gather(values, "ep", axis=0, tiled=True)
+    count = lax.axis_size("ep")
+    parts = jnp.stack([values for _ in range(count)])
+    parts = lax.all_to_all(parts, "ep", split_axis=0, concat_axis=0)
+    value_piece = jnp.concatenate(parts, axis=0)
     shard_count = key_piece.shape[0] // positions
     together = 1
     for candidate in (2, 3, 4):

time: 438 us -> 457 us (1.043)
  starting transfers between devices: 18.6 us -> 98.9 us
  waiting for transfers between devices: 187 us -> 122 us
    all_to_all x1, starting transfers between devices: 10.6 us -> 84.6 us  [local(): lax.all_to_all(summed, 'ep', split_axis=1, concat_axis=1, tiled=True)[0]]
    all_to_all x0 -> x1, waiting for transfers between devices: none -> 60.2 us  [local(): parts = lax.all_to_all(parts, 'ep', split_axis=0, concat_axis=0)]
    all_gather x1, waiting for transfers between devices: 55.6 us -> 0.02 us  [piecewise(): tiles = [lax.all_gather(section, axis) for section in pieces]]
    all_gather x1 -> x0, waiting for transfers between devices: 29.6 us -> none  [local(): value_piece = lax.all_gather(values, 'ep', axis=0, tiled=True)]
    all_gather x1, waiting for transfers between devices: 29.3 us -> 0.02 us  [local(): down_whole = lax.all_gather(w_down[0], 'tp', axis=0, tiled=True)]
    all_to_all x1, waiting for transfers between devices: 22.2 us -> 9.96 us  [local(): lax.all_to_all(hidden, 'tp', split_axis=0, concat_axis=3, tiled=True)]
    all_to_all x0 -> x1, starting transfers between devices: none -> 5.75 us  [local(): parts = lax.all_to_all(parts, 'ep', split_axis=0, concat_axis=0)]
    unnamed x22 -> x24, local copies, waits for them, and re-layouts: 28.1 us -> 28.2 us
  transfers between devices with their start and end apart: 7 -> 7, of which waited for: 5 -> 4; matrix products, arithmetic and copies ran while one was open for 28% -> 27% of each run, Pallas kernels for 0% -> 0%
where the time goes in v1:
time: 457 us; the launch traced here: 454 us
  waiting for transfers between devices  122 us (27%)
  local copies, waits for them, and re-layouts  101 us (22%)
  starting transfers between devices  98.9 us (22%)
  blocking collectives  73.1 us (16%)
  matrix products  22.8 us (5%)
  between operations  14.1 us (3%)
  other arithmetic  11.5 us (3%)
  loops' own time  9.72 us (2%)
    all_to_all x1, starting transfers between devices, local(): lax.all_to_all(summed, 'ep', split_axis=1, concat_axis=1, tiled=True)[0]  84.6 us
    all_to_all x1, blocking collectives, local(): lax.all_to_all(outgoing, 'ep', split_axis=0, concat_axis=0, tiled=True)  73.1 us
    all_to_all x1, waiting for transfers between devices, local(): parts = lax.all_to_all(parts, 'ep', split_axis=0, concat_axis=0)  60.2 us
    all_to_all x1, waiting for transfers between devices, local(): lax.all_to_all(summed, 'ep', split_axis=1, concat_axis=1, tiled=True)[0]  48.1 us
    scatter x1, local copies, waits for them, and re-layouts, fill_slots(): return (blank_slots.at[block_routes, slot_ids].set(copies), slot_ids)  33 us
    unnamed x24, local copies, waits for them, and re-layouts  28.2 us
    reshape x1, local copies, waits for them, and re-layouts, local(): key_blocks = key_piece.reshape(blocks, block_len, kv_heads, 2, head_dim)  14.8 us
    all_to_all x1, waiting for transfers between devices, local(): lax.all_to_all(hidden, 'tp', split_axis=0, concat_axis=3, tiled=True)  9.96 us
  transfers between devices with their start and end apart: 7, of which 4 were waited for; matrix products, arithmetic and copies ran while one was open for 27% of the time, Pallas kernels for 0%

profile of v1, /device:TPU:2, one launch (start us, length us, event | category | flops | bytes accessed | tf_op | source)
XLA Modules:
  0.0 453.6 jit_solution(12108201834496254006)
XLA Ops:
  7.2 0.7 all-gather.6.cloned.1.call-update
  8.0 0.7 constant_dynamic-slice_fusion
  9.1 0.6 reduce-window.6
  10.4 1.2 fusion.25
  11.6 1.3 fusion.27
  12.9 0.6 broadcast_in_dim.57
  13.5 1.2 reshape.246
  15.0 33.0 %scatter_fusion = bf16[64,8,2048]{2,1,0:T(8,128)(2,1)S(1)} fusion(bf16[64,8,2048]{2,1,0:T(8,128)(2,1)S(1)} %broadcast_in_dim.36, s32[256]{0:T(256)S(1)} %reshape.244, bf16[256,2048]{1,0:T(8,128)(2,1)} %reshape.246), kind=kCustom, calls=%fused_computation.1 | custom fusion | bytes 3147776 | tf_op jit(solution)/shard_map/scatter | solution.py:53
  48.0 73.1 %all_to_all.35 = bf16[64,8,2048]{2,1,0:T(8,128)(2,1)} all-to-all(bf16[64,8,2048]{2,1,0:T(8,128)(2,1)S(1)} %scatter_fusion), channel_id=1, replica_groups=mesh['ep'=64,'tp'=4] {'ep'}, dimensions={0} | all-to-all | bytes 4194304 | tf_op jit(solution)/shard_map/all_to_all | solution.py:174
  121.1 3.0 stack.2
  124.1 5.8 %all-to-all-start = ((bf16[64,256,1,128]{3,1,2,0:T(8,128)(2,1)}), bf16[64,256,1,128]{3,1,2,0:T(8,128)(2,1)}, u32[]{:S(2)}, u32[]{:S(2)}) async-start(bf16[64,256,1,128]{3,1,2,0:T(8,128)(2,1)} %stack.2), calls=%async_computation | async-start | bytes 8388608 | tf_op jit(solution)/shard_map/all_to_all | solution.py:89
  130.9 14.8 %reshape.262 = bf16[16,1024,1,2,64]{4,3,1,0,2:T(2,128)(2,1)} reshape(bf16[16384,1,128]{2,0,1:T(8,128)(2,1)} %all-gather.6.cloned.1.call-done) | data formatting | bytes 8388608 | tf_op jit(solution)/shard_map/reshape | solution.py:98
  145.6 20.2 %copy.37 = bf16[16,1024,1,2,64]{1,4,3,2,0:T(8,128)(2,1)} copy(bf16[16,1024,1,2,64]{4,3,1,0,2:T(2,128)(2,1)} %reshape.262) | data formatting | bytes 8388608
  165.8 60.2 %all-to-all-done = bf16[64,256,1,128]{3,1,2,0:T(8,128)(2,1)} async-done(((bf16[64,256,1,128]{3,1,2,0:T(8,128)(2,1)}), bf16[64,256,1,128]{3,1,2,0:T(8,128)(2,1)}, u32[]{:S(2)}, u32[]{:S(2)}) %all-to-all-start) | async-done | bytes 4194336 | tf_op jit(solution)/shard_map/all_to_all | solution.py:89
  226.0 6.4 %copy.39 = bf16[16,1024,1,128]{1,3,2,0:T(8,128)(2,1)} copy(bf16[16,1024,1,128]{3,1,0,2:T(8,128)(2,1)} %bitcast.18) | data formatting | bytes 8388608
  232.5 23.8 %while.15 = (s32[]{:T(128)}, f32[256,1,2,2]{0,2,3,1:T(2,128)S(1)}, f32[256,1,2,2]{0,2,3,1:T(2,128)S(1)}, f32[256,1,2,2,128]{0,4,3,2,1:T(8,128)S(1)}, s32[16]{0:T...) while((s32[]{:T(128)}, f32[256,1,2,2]{0,2,3,1:T(2,128)S(1)}, ...), condition=%wide.region_5.6_spmd.clone, body=%wide.region_0.5_spmd.clone.sunk | while | flops 411570432 | bytes 15156511 | solution.py:133
  233.6 5.2 %conditional.3 = ((f32[256,1,2,2]{0,2,3,1:T(2,128)S(1)}, f32[256,1,2,2]{0,2,3,1:T(2,128)S(1)}, f32[256,1,2,2,128]{0,4,3,2,1:T(8,128)S(1)})) conditional(s32[]{:T(128)} %convert_element_type.131, (f32[256,1,2,2]{0,2,3,1:T(2,128)S(1)}, f32[256,1,2,2]{0,2,3,1:T(2,128)S(1)}, f32[256,1,2,2,128]{0,4,3,2,1:T(8,128)S(1)}) %tuple.48, (s32[]{:T(128)}, ...), branch_computations={%region_1.1_spmd, %region_2.4_spmd} | conditional | flops 411570432 | bytes 15155240 | solution.py:131
  234.4 1.8 fusion.4
  236.3 1.0 fusion.5
  237.3 1.5 fusion.11
  240.0 0.6 dynamic_slice.56
  243.5 0.6 dynamic_slice.56
  244.6 0.6 dynamic_slice.56
  245.8 0.6 dynamic_slice.56
  248.1 0.6 dynamic_slice.56
  249.3 0.6 dynamic_slice.56
  250.4 0.6 dynamic_slice.56
  252.8 0.6 dynamic_slice.56
  256.4 5.9 %fusion.28 = f32[4,512,256]{2,1,0:T(8,128)S(1)} fusion(bf16[4,512,2048]{2,1,0:T(8,128)(2,1)} %bitcast.171, bf16[1,2048,256]{2,1,0:T(8,128)(2,1)S(1)} %copy-done), kind=kOutput, calls=%fused_computation.47 | convolution fusion | flops 2147483648 | bytes 11534336 | tf_op jit(solution)/shard_map/vmap()/dot_general | solution.py:162
  262.3 3.6 fusion.24
  266.0 4.5 all-to-all-start.3
  270.7 2.7 convolution_convert_fusion.4
  273.4 10.0 %all-to-all-done.3 = bf16[4,64,8,256]{3,2,1,0:T(8,128)(2,1)S(1)} async-done(((bf16[4,64,8,256]{3,2,1,0:T(8,128)(2,1)}), bf16[4,64,8,256]{3,2,1,0:T(8,128)(2,1)S(1)}, u32[]{:S(2)}, u32[]{:S(2)}) %all-to-all-start.3) | async-done | bytes 1048608 | tf_op jit(solution)/shard_map/all_to_all | solution.py:180
  283.4 3.7 all-to-all-start.1
  287.1 1.4 copy.65
  288.8 2.1 convolution_convert_fusion
  290.9 1.9 convolution_convert_fusion.1
  292.8 0.7 convolution_convert_fusion.2
  293.5 2.6 fusion.23
  296.1 2.6 all-to-all-done.1
  298.7 1.0 copy-done.2
  299.7 84.6 %all-to-all-start.4 = ((bf16[1,64,8,2048]{3,2,0,1:T(8,128)(2,1)}), bf16[1,64,8,2048]{3,2,0,1:T(8,128)(2,1)S(1)}, u32[]{:S(2)}, u32[]{:S(2)}) async-start(bf16[1,64,8,2048]{3,2,0,1:T(8,128)(2,1)} %fusion.23), calls=%async_computation.4 | async-start | bytes 4194304 | tf_op jit(solution)/shard_map/all_to_all | solution.py:192
  384.5 0.7 constant_dynamic-slice_fusion.1
  385.3 2.2 reduce_sum.60
  387.5 48.1 %all-to-all-done.4 = bf16[1,64,8,2048]{3,2,0,1:T(8,128)(2,1)S(1)} async-done(((bf16[1,64,8,2048]{3,2,0,1:T(8,128)(2,1)}), bf16[1,64,8,2048]{3,2,0,1:T(8,128)(2,1)S(1)}, u32[]{:S(2)}, u32[]{:S(2)}) %all-to-all-start.4) | async-done | bytes 2097184 | tf_op jit(solution)/shard_map/all_to_all | solution.py:192
  435.6 5.2 %gather_fusion = bf16[256,2048]{1,0:T(8,128)(2,1)} fusion(bf16[64,8,2048]{2,1,0:T(8,128)(2,1)S(1)} %bitcast.160, s32[256]{0:T(256)S(1)} %reshape.238), kind=kCustom, calls=%fused_computation | custom fusion | bytes 2099200 | tf_op jit(solution)/shard_map/gather | solution.py:193
  440.8 2.4 reshape.257
  443.2 3.9 multiply_reduce_fusion
  (100 shorter events, 8.9 us)
Async XLA Ops:
  7.2 249.2 %copy-start = (bf16[1,2048,256]{2,1,0:T(8,128)(2,1)S(1)}, bf16[1,2048,256]{2,1,0:T(8,128)(2,1)}, u32[]{:S(2)}) copy-start(bf16[1,2048,256]{2,1,0:T(8,128)(2,1)} %param.28) | copy-start | bytes 3145732
  7.2 123.7 %all-gather.6.cloned.1.call-start = ((), (), s32[]{:S(2)}) async-start(), calls=%async_computation.5 | async-start | bytes 4259840 | tf_op jit(solution)/shard_map/all_gather | solution.py:86
  7.9 248.4 %all-gather.8.cloned.1.call-start = ((), (), s32[]{:S(2)}) async-start(), calls=%async_computation.6 | async-start | bytes 10485760 | tf_op jit(solution)/shard_map/all_gather | solution.py:31
  48.0 73.1 %copy-start.4 = (bf16[256,1,128]{2,0,1:T(8,128)(2,1)S(1)}, bf16[256,1,128]{2,0,1:T(8,128)(2,1)}, u32[]{:S(2)}) copy-start(bf16[256,1,128]{2,0,1:T(8,128)(2,1)} %param.19) | copy-start | bytes 196612
  124.1 6.5 %copy-start.3 = (bf16[256,2,128]{2,1,0:T(2,128)(2,1)S(1)}, bf16[256,2,128]{2,1,0:T(2,128)(2,1)}, u32[]{:S(2)}) copy-start(bf16[256,2,128]{2,1,0:T(2,128)(2,1)} %param.17) | copy-start | bytes 393220
  124.1 6.7 %copy-start.5 = (f32[2]{0:T(128)S(1)}, f32[2]{0:T(128)}, u32[]{:S(2)}) copy-start(f32[2]{0:T(128)} %param.20) | copy-start | bytes 28
  124.1 6.7 %copy-start.6 = (f32[128]{0:T(128)S(1)}, f32[128]{0:T(128)}, u32[]{:S(2)}) copy-start(f32[128]{0:T(128)} %param.21) | copy-start | bytes 1540
  124.1 101.9 %all-to-all-start = ((bf16[64,256,1,128]{3,1,2,0:T(8,128)(2,1)}), bf16[64,256,1,128]{3,1,2,0:T(8,128)(2,1)}, u32[]{:S(2)}, u32[]{:S(2)}) async-start(bf16[64,256,1,128]{3,1,2,0:T(8,128)(2,1)} %stack.2), calls=%async_computation | async-start | bytes 8388608 | tf_op jit(solution)/shard_map/all_to_all | solution.py:89
  129.9 158.9 %all-gather.10.cloned.1.call-start = ((), (), s32[]{:S(2)}) async-start(), calls=%async_computation.7 | async-start | bytes 5242880 | tf_op jit(solution)/shard_map/all_gather | solution.py:181
  256.3 5.9 %copy-start.7 = (bf16[256,8,2048]{2,1,0:T(8,128)(2,1)S(1)}, bf16[256,8,2048]{2,1,0:T(8,128)(2,1)}, u32[]{:S(2)}) copy-start(bf16[256,8,2048]{2,1,0:T(8,128)(2,1)} %all-gather.8.cloned.1.call-done) | copy-start | bytes 25165828
  256.4 6.0 %copy-start.8 = (bf16[1,2048,256]{2,1,0:T(8,128)(2,1)S(1)}, bf16[1,2048,256]{2,1,0:T(8,128)(2,1)}, u32[]{:S(2)}) copy-start(bf16[1,2048,256]{2,1,0:T(8,128)(2,1)} %param.27) | copy-start | bytes 3145732
  266.0 17.4 %all-to-all-start.3 = ((bf16[4,64,8,256]{3,2,1,0:T(8,128)(2,1)}), bf16[4,64,8,256]{3,2,1,0:T(8,128)(2,1)S(1)}, u32[]{:S(2)}, u32[]{:S(2)}) async-start(bf16[4,64,8,256]{3,2,1,0:T(8,128)(2,1)} %fusion.24), calls=%async_computation.3 | async-start | bytes 2097152 | tf_op jit(solution)/shard_map/all_to_all | solution.py:180
  283.4 15.3 %all-to-all-start.1 = ((bf16[4,64,2048]{2,1,0:T(8,128)(2,1)}), bf16[4,64,2048]{2,1,0:T(8,128)(2,1)S(1)}, u32[]{:S(2)}, u32[]{:S(2)}) async-start(bf16[4,64,2048]{2,1,0:T(8,128)(2,1)} %bitcast.27), calls=%async_computation.1 | async-start | bytes 2097152 | tf_op jit(solution)/shard_map/all_to_all | solution.py:17
  288.8 4.1 copy-start.1
  298.7 1.0 copy-start.2
  299.7 135.9 %all-to-all-start.4 = ((bf16[1,64,8,2048]{3,2,0,1:T(8,128)(2,1)}), bf16[1,64,8,2048]{3,2,0,1:T(8,128)(2,1)S(1)}, u32[]{:S(2)}, u32[]{:S(2)}) async-start(bf16[1,64,8,2048]{3,2,0,1:T(8,128)(2,1)} %fusion.23), calls=%async_computation.4 | async-start | bytes 4194304 | tf_op jit(solution)/shard_map/all_to_all | solution.py:192
Sparse Core Ops, SparseCore 0:
  10.8 94.4 all-gather.5
  121.2 82.0 all-gather.7
  205.1 51.7 all-gather.9
